TPU v7x, 128 devices: a whole 4x4x4 slice. The times are simulated.
128 devices in a mesh: gr: 2 (over z_hi), fs: 32 (over z_lo, y, x), tp: 2 (over core).
Axes of the slice: x: 4, y: 4, z: 4 (z_hi: 2, z_lo: 2; z = z_hi * 2 + z_lo), core: 2. Of those that a mesh axis runs over, the one named last changes fastest.
Arguments:
- tokens: bfloat16 [4, 2048, 2048], P(('gr', 'tp')), may hold values from -6 to 6
- gate_master: float32 [3, 2048, 7168], P(None, 'fs', ('gr', 'tp')), may hold values from -0.125 to 0.125
- up_master: float32 [3, 2048, 7168], P(None, 'fs', ('gr', 'tp')), may hold values from -0.125 to 0.125
- down_master: float32 [3, 7168, 2048], P(None, 'fs', ('gr', 'tp')), may hold values from -0.0625 to 0.0625
- norm_gain: float32 [2048], P('fs'), may hold values from 0.1 to 1.9
- route: int32 [4, 2048, 2], P(('gr', 'tp')), may hold values from 0 to 2, all different within a row
- route_weight: float32 [4, 2048, 2], P(('gr', 'tp')), may hold values from 0.05 to 1
Outputs:
- gate_out: bfloat16 [3, 2048, 7168], P(None, None, 'fs')
- up_out: bfloat16 [3, 2048, 7168], P(None, None, 'fs')
- down_out: bfloat16 [3, 7168, 2048], P(None, 'fs')
- mixed: bfloat16 [4, 2048, 2048], P(('gr', 'tp'), 'fs')
Inputs may be any that keep to these rules, and one draw needn't show every extreme that they name: `route`: each token names two different experts; every expert is named by some token.
All inputs are finite; a program needn't handle non-finite values.
Results may differ from a plain program's by a relative error of at most 0.024.
Values may be sent and summed in bfloat16 or wider, within the bound.
No kernel may reach another device: no remote copies, remote signals or barrier semaphores. Data moves between devices by JAX's collectives and lax.ppermute only.
A program may use at most 192 MiB of HBM per device.

v0:
```python
import jax
import jax.numpy as jnp
from jax import lax
from jax.sharding import Mesh
from jax.sharding import PartitionSpec as P

FS = ("fs_0", "fs_1", "fs_2")


def reduced_to_own(blocks, axes, order):
    dims = [lax.axis_size(a) for a in axes]
    blocks = blocks.reshape(*dims, *blocks.shape[1:])
    blocks = blocks.transpose(*order, *range(len(axes), blocks.ndim))
    blocks = blocks.reshape(-1, *blocks.shape[len(axes) :])
    for k in order:
        blocks = lax.psum_scatter(blocks, axes[k], scatter_dimension=0, tiled=True)
    return blocks[0]


def split_up(array, dim, peers):
    dims = array.shape
    blocks = array.reshape(*dims[:dim], peers, dims[dim] // peers, *dims[dim + 1 :])
    return jnp.moveaxis(blocks, dim, 0)


def sum_by_axis_2(array, axes, order, dim):
    peers = lax.axis_size(axes)
    return reduced_to_own(split_up(array, dim, peers), axes, order)


def normalize(rows_in):
    values = rows_in.astype(jnp.float32)
    scaled = values * lax.rsqrt(jnp.mean(values * values, axis=-1, keepdims=True) + 1e-06)
    return scaled.astype(jnp.bfloat16)


def mixing(chosen, weights, experts):
    share = weights / jnp.sum(weights, axis=-1, keepdims=True)
    labels = jnp.arange(experts, dtype=jnp.int32)
    match = (chosen[:, :, None] == labels[None, None, :]).astype(jnp.float32)
    return jnp.sum(share[:, :, None] * match, axis=1)


def expert_term(normed, mix_column, gate_weight, up_weight, down_weight):
    gate_act = jnp.dot(normed, gate_weight, preferred_element_type=jnp.float32)
    up_act = jnp.dot(normed, up_weight, preferred_element_type=jnp.float32)
    hidden = (jax.nn.silu(gate_act) * up_act).astype(jnp.bfloat16)
    projected = jnp.dot(hidden, down_weight, preferred_element_type=jnp.float32)
    return mix_column * projected


def shards(tokens, gate_master, up_master, down_master, norm_gain, route, route_weight):
    scaled_gain = norm_gain[None, :, None]
    gate_local = (scaled_gain * gate_master).astype(jnp.bfloat16)
    up_local = (scaled_gain * up_master).astype(jnp.bfloat16)
    down_local = down_master.astype(jnp.bfloat16)
    experts = gate_local.shape[0]
    normed = normalize(tokens[0])
    combine = mixing(route[0], route_weight[0], experts)
    width = normed.shape[1]
    gate_rows, up_rows, down_out = (
        lax.all_gather(gate_local, ("gr", "tp"), axis=2, tiled=True),
        lax.all_gather(up_local, ("gr", "tp"), axis=2, tiled=True),
        lax.all_gather(down_local, ("gr", "tp"), axis=2, tiled=True),
    )
    gate_out, up_out = (
        lax.all_to_all(gate_rows, FS, split_axis=2, concat_axis=1, tiled=True),
        lax.all_to_all(up_rows, FS, split_axis=2, concat_axis=1, tiled=True),
    )
    own_rows = normed.shape[0] // lax.axis_size(FS)
    total = jnp.zeros((own_rows * lax.axis_size(FS), width), jnp.float32)
    for index in range(experts):
        total = total + expert_term(
            normed, combine[:, index : index + 1], gate_out[index], up_out[index], down_out[index]
        )
    summed = sum_by_axis_2(total.astype(jnp.bfloat16), FS, (1, 2, 0), 0).astype(jnp.float32)
    mixed = summed.astype(jnp.bfloat16)[None]
    return (gate_out, up_out, down_out, mixed)


def solution(mesh):
    split = Mesh(
        mesh.devices.reshape(mesh.shape["gr"], 2, 4, 4, mesh.shape["tp"]),
        ("gr", "fs_0", "fs_1", "fs_2", "tp"),
    )
    in_specs = (
        P(("gr", "tp"), None, None),
        P(None, FS, ("gr", "tp")),
        P(None, FS, ("gr", "tp")),
        P(None, FS, ("gr", "tp")),
        P(FS),
        P(("gr", "tp"), None, None),
        P(("gr", "tp"), None, None),
    )
    out_specs = (P(None, None, FS), P(None, None, FS), P(None, FS, None), P(("gr", "tp"), FS, None))
    return jax.shard_map(
        shards, mesh=split, in_specs=in_specs, out_specs=out_specs, check_vma=False
    )
```

profile of v0, /device:TPU:1, one launch (start us, length us, event | category | flops | bytes accessed | tf_op | source)
XLA Modules:
  0.0 390.9 jit_solution(5299467397481243480)
XLA Ops:
  11.1 33.5 %all-gather.4.cloned.1.call-done = bf16[3,64,7168]{2,1,0:T(8,128)(2,1)} async-done(((bf16[3,64,1792]{2,1,0:T(8,128)(2,1)}), bf16[3,64,7168]{2,1,0:T(8,128)(2,1)}) %all-gather.4.cloned.1.call-update) | async-done | bytes 2752528 | tf_op jit(solution)/shard_map/all_gather | solution.py:62
  44.5 10.1 %copy.41 = bf16[3,64,7168]{1,0,2:T(4,128)(2,1)} copy(bf16[3,64,7168]{2,1,0:T(8,128)(2,1)} %all-gather.4.cloned.1.call-done) | data formatting | bytes 5505024 | tf_op jit(solution)/shard_map/all_gather | solution.py:62
  54.6 12.6 %reshape.105 = bf16[32,2,21504]{2,1,0:T(2,128)(2,1)} reshape(bf16[7168,3,64]{2,1,0:T(4,128)(2,1)} %bitcast.55) | data formatting | bytes 5505024
  67.2 7.0 %all-to-all-start = ((bf16[32,2,21504]{2,1,0:T(2,128)(2,1)}), bf16[32,2,21504]{2,1,0:T(2,128)(2,1)S(1)}, u32[]{:S(2)}, u32[]{:S(2)}) async-start(bf16[32,2,21504]{2,1,0:T(2,128)(2,1)} %reshape.105), calls=%async_computation | async-start | bytes 5505024 | tf_op jit(solution)/shard_map/all_to_all | solution.py:67
  76.7 10.1 %copy.43 = bf16[3,64,7168]{1,0,2:T(4,128)(2,1)} copy(bf16[3,64,7168]{2,1,0:T(8,128)(2,1)} %all-gather.6.cloned.1.call-done) | data formatting | bytes 5505024 | tf_op jit(solution)/shard_map/all_gather | solution.py:63
  86.8 12.6 %reshape.107 = bf16[32,2,21504]{2,1,0:T(2,128)(2,1)} reshape(bf16[7168,3,64]{2,1,0:T(4,128)(2,1)} %bitcast.56) | data formatting | bytes 5505024
  99.4 9.2 %all-to-all-done = bf16[32,2,21504]{2,1,0:T(2,128)(2,1)S(1)} async-done(((bf16[32,2,21504]{2,1,0:T(2,128)(2,1)}), bf16[32,2,21504]{2,1,0:T(2,128)(2,1)S(1)}, u32[]{:S(2)}, u32[]{:S(2)}) %all-to-all-start) | async-done | bytes 2752544 | tf_op jit(solution)/shard_map/all_to_all | solution.py:67
  108.6 6.3 %all-to-all-start.1 = ((bf16[32,2,21504]{2,1,0:T(2,128)(2,1)}), bf16[32,2,21504]{2,1,0:T(2,128)(2,1)}, u32[]{:S(2)}, u32[]{:S(2)}) async-start(bf16[32,2,21504]{2,1,0:T(2,128)(2,1)} %reshape.107), calls=%async_computation.1 | async-start | bytes 5505024 | tf_op jit(solution)/shard_map/all_to_all | solution.py:68
  115.1 5.1 %fusion = f32[2048]{0:T(1024)S(1)} fusion(bf16[1,2048,2048]{2,1,0:T(8,128)(2,1)} %param.7), kind=kLoop, calls=%fused_computation.2 | loop fusion | flops 12580864 | bytes 8396800 | tf_op jit(solution)/shard_map/reduce_sum | solution.py:33
  120.3 8.0 %fusion.2 = bf16[2048,2048]{1,0:T(8,128)(2,1)} fusion(bf16[1,2048,2048]{2,1,0:T(8,128)(2,1)} %param.7, f32[2048]{0:T(1024)S(1)} %add_rsqrt_fusion), kind=kLoop, calls=%fused_computation.5 | loop fusion | flops 12582912 | bytes 16785408 | tf_op jit(solution)/shard_map/convert_element_type | solution.py:34
  128.3 8.7 %reshape.106 = bf16[7168,3,64]{2,1,0:T(4,128)(2,1)} reshape(bf16[32,2,21504]{2,1,0:T(2,128)(2,1)S(1)} %all-to-all-done) | data formatting | bytes 5505024
  136.9 10.7 %copy.42 = bf16[3,64,32,224]{3,1,2,0:T(8,128)(2,1)S(1)} copy(bf16[3,64,32,224]{1,0,3,2:T(4,128)(2,1)} %bitcast.57) | data formatting | bytes 5505024 | tf_op jit(solution)/shard_map/all_to_all | solution.py:67
  148.6 12.5 %reshape.108 = bf16[7168,3,64]{2,1,0:T(4,128)(2,1)} reshape(bf16[32,2,21504]{2,1,0:T(2,128)(2,1)} %all-to-all-done.1) | data formatting | bytes 5505024
  161.0 11.4 %copy.44 = bf16[3,64,32,224]{3,1,2,0:T(8,128)(2,1)} copy(bf16[3,64,32,224]{1,0,3,2:T(4,128)(2,1)} %bitcast.58) | data formatting | bytes 5505024 | tf_op jit(solution)/shard_map/all_to_all | solution.py:68
  176.1 8.0 %fusion.27 = f32[2048,224]{0,1:T(8,128)} fusion(bf16[2048,2048]{1,0:T(8,128)(2,1)} %fusion.2, bf16[2048,224]{1,0:T(8,128)(2,1)S(1)} %bitcast.68), kind=kOutput, calls=%fused_computation.41 | convolution fusion | flops 1879048192 | bytes 11141120 | tf_op jit(solution)/shard_map/dot_general | solution.py:45
  188.1 4.0 %fusion.29 = f32[2048,224]{0,1:T(8,128)} fusion(bf16[2048,2048]{1,0:T(8,128)(2,1)S(1)} %bitcast.52, bf16[2048,224]{1,0:T(8,128)(2,1)S(1)} %bitcast.66), kind=kOutput, calls=%fused_computation.43 | convolution fusion | flops 1879048192 | bytes 11141120 | tf_op jit(solution)/shard_map/dot_general | solution.py:45
  192.1 15.3 %fusion.7 = f32[2048,2048]{1,0:T(8,128)} fusion(bf16[2048,2048]{1,0:T(8,128)(2,1)} %fusion.2, bf16[2048,224]{1,0:T(8,128)(2,1)} %bitcast.64, f32[2048,224]{0,1:T(8,128)} %fusion.27, bf16[3,224,2048]{2,1,0:T(8,128)(2,1)} %all-gather.8.cloned.1.call-done), kind=kOutput, calls=%fused_computation.13 | convolution fusion | flops 3760848896 | bytes 28966912 | tf_op jit(solution)/shard_map/dot_general | solution.py:48
  207.4 15.5 %fusion.6 = f32[2048,2048]{1,0:T(8,128)} fusion(bf16[2048,2048]{1,0:T(8,128)(2,1)} %fusion.2, bf16[2048,224]{1,0:T(8,128)(2,1)} %bitcast.63, f32[2048,224]{0,1:T(8,128)} %fusion.28, bf16[3,224,2048]{2,1,0:T(8,128)(2,1)} %all-gather.8.cloned.1.call-done), kind=kOutput, calls=%fused_computation.12 | convolution fusion | flops 3760848896 | bytes 28966912 | tf_op jit(solution)/shard_map/dot_general | solution.py:48
  222.9 19.2 %add_convert_fusion = bf16[2048,2048]{1,0:T(8,128)(2,1)} fusion(f32[2048,2048]{1,0:T(8,128)} %fusion.6, f32[2048,2048]{1,0:T(8,128)} %fusion.7, f32[2048]{0:T(1024)S(1)} %bitcast.70, f32[2048]{0:T(1024)S(1)} %bitcast.71, f32[2048]{0:T(1024)S(1)} %bitcast.69, bf16[3,224,2048]{2,1,0:T(8,128)(2,1)} %all-gather.8.cloned.1.call-done, ...), kind=kOutput, calls=%fused_computation.4 | convolution fusion | flops 3786014720 | bytes 54157312 | tf_op jit(solution)/shard_map/dot_general | solution.py:48
  242.0 8.3 %copy.45 = bf16[4,4,2,64,2048]{4,3,2,1,0:T(8,128)(2,1)} copy(bf16[4,4,2,64,2048]{4,3,1,0,2:T(8,128)(2,1)} %bitcast.54) | data formatting | bytes 16777216 | tf_op jit(solution)/shard_map/transpose | solution.py:13
  250.4 80.8 %reduce-scatter.4.cloned.1.call-done = bf16[8,64,2048]{2,1,0:T(8,128)(2,1)} async-done(((bf16[32,64,2048]{2,1,0:T(8,128)(2,1)}), bf16[8,64,2048]{2,1,0:T(8,128)(2,1)}) %reduce-scatter.4.cloned.1.call-update) | async-done | bytes 2097168 | tf_op jit(solution)/shard_map/reduce_scatter | solution.py:16
  331.3 31.6 %reduce-scatter.6.cloned.1.call-done = bf16[2,64,2048]{2,1,0:T(8,128)(2,1)} async-done(((bf16[8,64,2048]{2,1,0:T(8,128)(2,1)}), bf16[2,64,2048]{2,1,0:T(8,128)(2,1)}) %reduce-scatter.6.cloned.1.call-update) | async-done | bytes 524304 | tf_op jit(solution)/shard_map/reduce_scatter | solution.py:16
  365.6 4.7 %copy.47 = bf16[3,2048,224]{1,2,0:T(8,128)(2,1)} copy(bf16[3,2048,224]{2,1,0:T(8,128)(2,1)} %bitcast.61) | data formatting | bytes 5505024
  370.3 12.2 %reduce-scatter.8.cloned.1.call-done = bf16[1,64,2048]{2,1,0:T(8,128)(2,1)} async-done(((bf16[2,64,2048]{2,1,0:T(8,128)(2,1)}), bf16[1,64,2048]{2,1,0:T(8,128)(2,1)}) %reduce-scatter.8.cloned.1.call-update) | async-done | bytes 262160 | tf_op jit(solution)/shard_map/reduce_scatter | solution.py:16
  (40 shorter events, 19.4 us)
Async XLA Ops:
  7.2 37.4 %all-gather.4.cloned.1.call-start = ((), (), s32[]{:S(2)}) async-start(), calls=%async_computation.5 | async-start | bytes 3440640 | tf_op jit(solution)/shard_map/all_gather | solution.py:62
  10.3 66.4 %all-gather.6.cloned.1.call-start = ((), (), s32[]{:S(2)}) async-start(), calls=%async_computation.6 | async-start | bytes 3440640 | tf_op jit(solution)/shard_map/all_gather | solution.py:63
  67.2 41.4 %all-to-all-start = ((bf16[32,2,21504]{2,1,0:T(2,128)(2,1)}), bf16[32,2,21504]{2,1,0:T(2,128)(2,1)S(1)}, u32[]{:S(2)}, u32[]{:S(2)}) async-start(bf16[32,2,21504]{2,1,0:T(2,128)(2,1)} %reshape.105), calls=%async_computation | async-start | bytes 5505024 | tf_op jit(solution)/shard_map/all_to_all | solution.py:67
  74.3 2.4 copy-start.2
  74.3 117.9 %all-gather.8.cloned.1.call-start = ((), (), s32[]{:S(2)}) async-start(), calls=%async_computation.7 | async-start | bytes 3440640 | tf_op jit(solution)/shard_map/all_gather | solution.py:64
  99.4 15.6 %copy-start.3 = (s32[1,2048,2]{1,2,0:T(2,128)S(1)}, s32[1,2048,2]{1,2,0:T(2,128)}, u32[]{:S(2)}) copy-start(s32[1,2048,2]{1,2,0:T(2,128)} %param.12) | copy-start | bytes 49156
  108.6 39.9 %all-to-all-start.1 = ((bf16[32,2,21504]{2,1,0:T(2,128)(2,1)}), bf16[32,2,21504]{2,1,0:T(2,128)(2,1)}, u32[]{:S(2)}, u32[]{:S(2)}) async-start(bf16[32,2,21504]{2,1,0:T(2,128)(2,1)} %reshape.107), calls=%async_computation.1 | async-start | bytes 5505024 | tf_op jit(solution)/shard_map/all_to_all | solution.py:68
  115.0 216.3 %reduce-scatter.4.cloned.1.call-start = ((), (), s32[]{:S(2)}) async-start(), calls=%async_computation.8 | async-start | bytes 10485760 | tf_op jit(solution)/shard_map/reduce_scatter | solution.py:16
  172.4 1.9 copy-start
  174.3 9.8 %slice-start = ((s8[8388608]{0:T(1024)(128)(4,1)}), s8[4194304]{0:T(1024)(128)(4,1)S(1)}, s32[]{:S(2)}) async-start(s8[8388608]{0:T(1024)(128)(4,1)} %bitcast.51), calls=%async_computation.11 | async-start | bytes 8388608
  176.1 8.0 %slice-start.1 = ((s8[8388608]{0:T(1024)(128)(4,1)}), s8[4194304]{0:T(1024)(128)(4,1)S(1)}, s32[]{:S(2)}) async-start(s8[8388608]{0:T(1024)(128)(4,1)} %bitcast.51), calls=%async_computation.12 | async-start | bytes 8388608
  250.3 112.5 %reduce-scatter.6.cloned.1.call-start = ((), (), s32[]{:S(2)}) async-start(), calls=%async_computation.9 | async-start | bytes 2621440 | tf_op jit(solution)/shard_map/reduce_scatter | solution.py:16
  331.2 51.3 %reduce-scatter.8.cloned.1.call-start = ((), (), s32[]{:S(2)}) async-start(), calls=%async_computation.10 | async-start | bytes 786432 | tf_op jit(solution)/shard_map/reduce_scatter | solution.py:16
  365.6 16.9 %copy-start.1 = (bf16[3,224,2048]{2,1,0:T(8,128)(2,1)S(1)}, bf16[3,224,2048]{2,1,0:T(8,128)(2,1)}, u32[]{:S(2)}) copy-start(bf16[3,224,2048]{2,1,0:T(8,128)(2,1)} %all-gather.8.cloned.1.call-done) | copy-start | bytes 8257540
Sparse Core Ops, SparseCore 0:
  10.4 34.0 all-gather.3
  46.8 29.6 all-gather.5
  78.1 74.4 all-gather.7
  250.5 80.7 reduce-scatter.3
  333.5 29.3 reduce-scatter.5
  365.6 16.8 reduce-scatter.7
where the time goes:
time: 393 us; the launch traced here: 391 us
  waiting for transfers between devices  169 us (43%)
  local copies, waits for them, and re-layouts  110 us (28%)
  matrix products  65.9 us (17%)
  other arithmetic  18.6 us (5%)
  between operations  14.2 us (4%)
  starting transfers between devices  13.6 us (3%)
    reduce_scatter x3, waiting for transfers between devices, reduced_to_own(): blocks = lax.psum_scatter(blocks, axes[k], scatter_dimension=0, tiled=True)  125 us
    unnamed x19, local copies, waits for them, and re-layouts  57 us
    dot_general x3, matrix products, expert_term(): projected = jnp.dot(hidden, down_weight, preferred_element_type=jnp.float32)  49.9 us
    all_gather x1, waiting for transfers between devices, shards(): lax.all_gather(gate_local, ('gr', 'tp'), axis=2, tiled=True)  33.5 us
    dot_general x3, matrix products, expert_term(): gate_act = jnp.dot(normed, gate_weight, preferred_element_type=jnp.float32)  16 us
    all_to_all x1, local copies, waits for them, and re-layouts, shards(): lax.all_to_all(up_rows, FS, split_axis=2, concat_axis=1, tiled=True)  11.4 us
    all_to_all x1, local copies, waits for them, and re-layouts, shards(): lax.all_to_all(gate_rows, FS, split_axis=2, concat_axis=1, tiled=True)  10.7 us
    all_gather x1, local copies, waits for them, and re-layouts, shards(): lax.all_gather(up_local, ('gr', 'tp'), axis=2, tiled=True)  10.1 us
  transfers between devices with their start and end apart: 8, of which 6 were waited for; matrix products, arithmetic and copies ran while one was open for 33% of the time, Pallas kernels for 0%

commit v1 on v0

--- a/solution.py
+++ b/solution.py
@@ -1,3 +1,4 @@
+import functools
 import jax
 import jax.numpy as jnp
 from jax import lax
@@ -5,6 +6,15 @@
 from jax.sharding import PartitionSpec as P
 
 FS = ("fs_0", "fs_1", "fs_2")
+
+
+def wrap_the_modes(m, dim_i, axis_no):
+    return jnp.concatenate(
+        lax.all_to_all(jnp.stack(jnp.split(m, lax.axis_size(FS), dim_i), 0), FS, 0, 0), axis_no
+    )
+
+
+enter_the_clusters = functools.partial(wrap_the_modes, dim_i=2, axis_no=1)
 
 
 def reduced_to_own(blocks, axes, order):
@@ -64,7 +74,7 @@
         lax.all_gather(down_local, ("gr", "tp"), axis=2, tiled=True),
     )
     gate_out, up_out = (
-        lax.all_to_all(gate_rows, FS, split_axis=2, concat_axis=1, tiled=True),
+        enter_the_clusters(gate_rows),
         lax.all_to_all(up_rows, FS, split_axis=2, concat_axis=1, tiled=True),
     )
     own_rows = normed.shape[0] // lax.axis_size(FS)

time: 393 us -> 383 us (0.975)
  waiting for transfers between devices: 169 us -> 159 us
    all_gather x1, waiting for transfers between devices: 0.02 us -> 32.4 us  [shards(): lax.all_gather(up_local, ('gr', 'tp'), axis=2, tiled=True)]
    all_gather x1, waiting for transfers between devices: 33.5 us -> 2.23 us  [shards(): lax.all_gather(gate_local, ('gr', 'tp'), axis=2, tiled=True)]
    unnamed x19 -> x54, local copies, waits for them, and re-layouts: 57 us -> 76 us
    all_to_all x1 -> x0, local copies, waits for them, and re-layouts: 10.7 us -> none  [shards(): lax.all_to_all(gate_rows, FS, split_axis=2, concat_axis=1, tiled=True)]
    all_gather x1 -> x0, local copies, waits for them, and re-layouts: 10.1 us -> none  [shards(): lax.all_gather(gate_local, ('gr', 'tp'), axis=2, tiled=True)]
    all_to_all x1, waiting for transfers between devices: 9.23 us -> 1.97 us  [wrap_the_modes(): lax.all_to_all(jnp.stack(jnp.split(m, lax.axis_size(FS), dim_i), 0), FS,...]
where the time goes in v1:
time: 383 us; the launch traced here: 381 us
  waiting for transfers between devices  159 us (42%)
  local copies, waits for them, and re-layouts  110 us (29%)
  matrix products  65.9 us (17%)
  other arithmetic  17.4 us (5%)
  starting transfers between devices  14.2 us (4%)
  between operations  14.2 us (4%)
    reduce_scatter x3, waiting for transfers between devices, reduced_to_own(): blocks = lax.psum_scatter(blocks, axes[k], scatter_dimension=0, tiled=True)  122 us
    unnamed x54, local copies, waits for them, and re-layouts  76 us
    dot_general x3, matrix products, expert_term(): projected = jnp.dot(hidden, down_weight, preferred_element_type=jnp.float32)  49.9 us
    all_gather x1, waiting for transfers between devices, shards(): lax.all_gather(up_local, ('gr', 'tp'), axis=2, tiled=True)  32.4 us
    dot_general x3, matrix products, expert_term(): gate_act = jnp.dot(normed, gate_weight, preferred_element_type=jnp.float32)  16 us
    all_to_all x1, local copies, waits for them, and re-layouts, shards(): lax.all_to_all(up_rows, FS, split_axis=2, concat_axis=1, tiled=True)  11.3 us
    all_gather x1, local copies, waits for them, and re-layouts, shards(): lax.all_gather(up_local, ('gr', 'tp'), axis=2, tiled=True)  10 us
    transpose x1, local copies, waits for them, and re-layouts, reduced_to_own(): blocks = blocks.transpose(*order, *range(len(axes), blocks.ndim))  8.28 us
  transfers between devices with their start and end apart: 8, of which 6 were waited for; matrix products, arithmetic and copies ran while one was open for 33% of the time, Pallas kernels for 0%

profile of v1, /device:TPU:1, one launch (start us, length us, event | category | flops | bytes accessed | tf_op | source)
XLA Modules:
  0.0 381.5 jit_solution(254166681760322126)
XLA Ops:
  7.2 3.2 multiply_convert_fusion
  12.3 32.4 %all-gather.6.cloned.1.call-done = bf16[3,64,7168]{2,1,0:T(8,128)(2,1)} async-done(((bf16[3,64,1792]{2,1,0:T(8,128)(2,1)}), bf16[3,64,7168]{2,1,0:T(8,128)(2,1)}) %all-gather.6.cloned.1.call-update) | async-done | bytes 2752528 | tf_op jit(solution)/shard_map/all_gather | solution.py:73
  44.6 10.0 %copy.53 = bf16[3,64,7168]{1,0,2:T(4,128)(2,1)} copy(bf16[3,64,7168]{2,1,0:T(8,128)(2,1)} %all-gather.6.cloned.1.call-done) | data formatting | bytes 5505024 | tf_op jit(solution)/shard_map/all_gather | solution.py:73
  54.7 12.6 %reshape.113 = bf16[32,2,21504]{2,1,0:T(2,128)(2,1)} reshape(bf16[7168,3,64]{2,1,0:T(4,128)(2,1)} %bitcast.179) | data formatting | bytes 5505024
  67.3 7.0 %all-to-all-start.1 = ((bf16[32,2,21504]{2,1,0:T(2,128)(2,1)}), bf16[32,2,21504]{2,1,0:T(2,128)(2,1)S(1)}, u32[]{:S(2)}, u32[]{:S(2)}) async-start(bf16[32,2,21504]{2,1,0:T(2,128)(2,1)} %reshape.113), calls=%async_computation.1 | async-start | bytes 5505024 | tf_op jit(solution)/shard_map/all_to_all | solution.py:78
  74.3 2.2 all-gather.4.cloned.1.call-done
  115.6 6.9 %all-to-all-start = ((bf16[32,3,64,224]{3,2,1,0:T(8,128)(2,1)}), bf16[32,3,64,224]{3,2,1,0:T(8,128)(2,1)S(1)}, u32[]{:S(2)}, u32[]{:S(2)}) async-start(bf16[32,3,64,224]{3,2,1,0:T(8,128)(2,1)} %fusion.20), calls=%async_computation | async-start | bytes 6291456 | tf_op jit(solution)/shard_map/all_to_all | solution.py:13
  122.6 5.1 %fusion = f32[2048]{0:T(1024)S(1)} fusion(bf16[1,2048,2048]{2,1,0:T(8,128)(2,1)} %param.7), kind=kLoop, calls=%fused_computation.2 | loop fusion | flops 12580864 | bytes 8396800 | tf_op jit(solution)/shard_map/reduce_sum | solution.py:43
  127.7 8.0 %fusion.2 = bf16[2048,2048]{1,0:T(8,128)(2,1)} fusion(bf16[1,2048,2048]{2,1,0:T(8,128)(2,1)} %param.7, f32[2048]{0:T(1024)S(1)} %add_rsqrt_fusion), kind=kLoop, calls=%fused_computation.5 | loop fusion | flops 12582912 | bytes 16785408 | tf_op jit(solution)/shard_map/convert_element_type | solution.py:44
  135.8 12.4 %reshape.114 = bf16[7168,3,64]{2,1,0:T(4,128)(2,1)} reshape(bf16[32,2,21504]{2,1,0:T(2,128)(2,1)} %copy-done.2) | data formatting | bytes 5505024
  148.2 11.3 %copy.54 = bf16[3,64,32,224]{3,1,2,0:T(8,128)(2,1)} copy(bf16[3,64,32,224]{1,0,3,2:T(4,128)(2,1)} %bitcast.180) | data formatting | bytes 5505024 | tf_op jit(solution)/shard_map/all_to_all | solution.py:78
  165.3 8.0 %fusion.60 = f32[2048,224]{0,1:T(8,128)} fusion(bf16[2048,2048]{1,0:T(8,128)(2,1)} %fusion.2, bf16[2048,224]{1,0:T(8,128)(2,1)S(1)} %bitcast.191), kind=kOutput, calls=%fused_computation.106 | convolution fusion | flops 1879048192 | bytes 11141120 | tf_op jit(solution)/shard_map/dot_general | solution.py:55
  173.2 4.0 %fusion.59 = f32[2048,224]{0,1:T(8,128)} fusion(bf16[2048,2048]{1,0:T(8,128)(2,1)S(1)} %bitcast.176, bf16[2048,224]{1,0:T(8,128)(2,1)S(1)} %bitcast.190), kind=kOutput, calls=%fused_computation.105 | convolution fusion | flops 1879048192 | bytes 11141120 | tf_op jit(solution)/shard_map/dot_general | solution.py:55
  177.3 4.0 %fusion.61 = f32[2048,224]{0,1:T(8,128)} fusion(bf16[2048,2048]{1,0:T(8,128)(2,1)S(1)} %bitcast.176, bf16[2048,224]{1,0:T(8,128)(2,1)S(1)} %bitcast.189), kind=kOutput, calls=%fused_computation.107 | convolution fusion | flops 1879048192 | bytes 11141120 | tf_op jit(solution)/shard_map/dot_general | solution.py:55
  181.3 15.2 %fusion.6 = f32[2048,2048]{1,0:T(8,128)} fusion(bf16[2048,2048]{1,0:T(8,128)(2,1)} %fusion.2, bf16[2048,224]{1,0:T(8,128)(2,1)} %bitcast.187, f32[2048,224]{0,1:T(8,128)} %fusion.60, bf16[3,224,2048]{2,1,0:T(8,128)(2,1)} %all-gather.8.cloned.1.call-done), kind=kOutput, calls=%fused_computation.12 | convolution fusion | flops 3760848896 | bytes 28966912 | tf_op jit(solution)/shard_map/dot_general | solution.py:58
  196.5 15.5 %fusion.7 = f32[2048,2048]{1,0:T(8,128)} fusion(bf16[2048,2048]{1,0:T(8,128)(2,1)} %fusion.2, bf16[2048,224]{1,0:T(8,128)(2,1)} %bitcast.186, f32[2048,224]{0,1:T(8,128)} %fusion.59, bf16[3,224,2048]{2,1,0:T(8,128)(2,1)} %all-gather.8.cloned.1.call-done), kind=kOutput, calls=%fused_computation.13 | convolution fusion | flops 3760848896 | bytes 28966912 | tf_op jit(solution)/shard_map/dot_general | solution.py:58
  212.0 19.2 %add_convert_fusion = bf16[2048,2048]{1,0:T(8,128)(2,1)} fusion(f32[2048,2048]{1,0:T(8,128)} %fusion.6, f32[2048,2048]{1,0:T(8,128)} %fusion.7, f32[2048]{0:T(1024)S(1)} %bitcast.193, f32[2048]{0:T(1024)S(1)} %bitcast.194, f32[2048]{0:T(1024)S(1)} %bitcast.192, bf16[3,224,2048]{2,1,0:T(8,128)(2,1)} %all-gather.8.cloned.1.call-done, ...), kind=kOutput, calls=%fused_computation.4 | convolution fusion | flops 3786014720 | bytes 54157312 | tf_op jit(solution)/shard_map/dot_general | solution.py:58
  231.2 8.3 %copy.55 = bf16[4,4,2,64,2048]{4,3,2,1,0:T(8,128)(2,1)} copy(bf16[4,4,2,64,2048]{4,3,1,0,2:T(8,128)(2,1)} %bitcast.178) | data formatting | bytes 16777216 | tf_op jit(solution)/shard_map/transpose | solution.py:23
  239.5 80.2 %reduce-scatter.4.cloned.1.call-done = bf16[8,64,2048]{2,1,0:T(8,128)(2,1)} async-done(((bf16[32,64,2048]{2,1,0:T(8,128)(2,1)}), bf16[8,64,2048]{2,1,0:T(8,128)(2,1)}) %reduce-scatter.4.cloned.1.call-update) | async-done | bytes 2097168 | tf_op jit(solution)/shard_map/reduce_scatter | solution.py:26
  319.7 31.6 %reduce-scatter.6.cloned.1.call-done = bf16[2,64,2048]{2,1,0:T(8,128)(2,1)} async-done(((bf16[8,64,2048]{2,1,0:T(8,128)(2,1)}), bf16[2,64,2048]{2,1,0:T(8,128)(2,1)}) %reduce-scatter.6.cloned.1.call-update) | async-done | bytes 524304 | tf_op jit(solution)/shard_map/reduce_scatter | solution.py:26
  353.2 4.7 %copy.56 = bf16[3,2048,224]{1,2,0:T(8,128)(2,1)} copy(bf16[3,2048,224]{2,1,0:T(8,128)(2,1)} %bitcast.185) | data formatting | bytes 5505024
  357.9 2.7 copy.57
  360.6 10.4 %reduce-scatter.8.cloned.1.call-done = bf16[1,64,2048]{2,1,0:T(8,128)(2,1)} async-done(((bf16[2,64,2048]{2,1,0:T(8,128)(2,1)}), bf16[1,64,2048]{2,1,0:T(8,128)(2,1)}) %reduce-scatter.8.cloned.1.call-update) | async-done | bytes 262160 | tf_op jit(solution)/shard_map/reduce_scatter | solution.py:26
  371.0 3.7 copy.90
  (75 shorter events, 48.6 us)
Async XLA Ops:
  7.2 4.1 %copy-start.4 = (f32[3,224,512]{2,1,0:T(8,128)S(1)}, f32[3,224,512]{2,1,0:T(8,128)}, u32[]{:S(2)}) copy-start(f32[3,224,512]{2,1,0:T(8,128)} %param.10) | copy-start | bytes 4128772
  7.2 5.0 %copy-start.5 = (f32[1,2048,2]{1,2,0:T(2,128)S(1)}, f32[1,2048,2]{1,2,0:T(2,128)}, u32[]{:S(2)}) copy-start(f32[1,2048,2]{1,2,0:T(2,128)} %param.13) | copy-start | bytes 49156
  7.2 37.5 %all-gather.6.cloned.1.call-start = ((), (), s32[]{:S(2)}) async-start(), calls=%async_computation.6 | async-start | bytes 3440640 | tf_op jit(solution)/shard_map/all_gather | solution.py:73
  10.4 66.2 %all-gather.4.cloned.1.call-start = ((), (), s32[]{:S(2)}) async-start(), calls=%async_computation.5 | async-start | bytes 3440640 | tf_op jit(solution)/shard_map/all_gather | solution.py:72
  11.2 170.1 %all-gather.8.cloned.1.call-start = ((), (), s32[]{:S(2)}) async-start(), calls=%async_computation.7 | async-start | bytes 3440640 | tf_op jit(solution)/shard_map/all_gather | solution.py:74
  67.3 46.7 %all-to-all-start.1 = ((bf16[32,2,21504]{2,1,0:T(2,128)(2,1)}), bf16[32,2,21504]{2,1,0:T(2,128)(2,1)S(1)}, u32[]{:S(2)}, u32[]{:S(2)}) async-start(bf16[32,2,21504]{2,1,0:T(2,128)(2,1)} %reshape.113), calls=%async_computation.1 | async-start | bytes 5505024 | tf_op jit(solution)/shard_map/all_to_all | solution.py:78
  76.6 26.0 %copy-start.3 = (bf16[3,64,7168]{2,1,0:T(8,128)(2,1)S(1)}, bf16[3,64,7168]{2,1,0:T(8,128)(2,1)}, u32[]{:S(2)}) copy-start(bf16[3,64,7168]{2,1,0:T(8,128)(2,1)} %all-gather.4.cloned.1.call-done) | copy-start | bytes 8257540
  114.0 8.5 %copy-start.6 = (s32[1,2048,2]{1,2,0:T(2,128)S(1)}, s32[1,2048,2]{1,2,0:T(2,128)}, u32[]{:S(2)}) copy-start(s32[1,2048,2]{1,2,0:T(2,128)} %param.12) | copy-start | bytes 49156
  114.0 1.5 copy-start.2
  115.6 46.0 %all-to-all-start = ((bf16[32,3,64,224]{3,2,1,0:T(8,128)(2,1)}), bf16[32,3,64,224]{3,2,1,0:T(8,128)(2,1)S(1)}, u32[]{:S(2)}, u32[]{:S(2)}) async-start(bf16[32,3,64,224]{3,2,1,0:T(8,128)(2,1)} %fusion.20), calls=%async_computation | async-start | bytes 6291456 | tf_op jit(solution)/shard_map/all_to_all | solution.py:13
  122.5 197.2 %reduce-scatter.4.cloned.1.call-start = ((), (), s32[]{:S(2)}) async-start(), calls=%async_computation.8 | async-start | bytes 10485760 | tf_op jit(solution)/shard_map/reduce_scatter | solution.py:26
  161.5 1.9 copy-start
  163.4 9.8 %slice-start = ((s8[8388608]{0:T(1024)(128)(4,1)}), s8[4194304]{0:T(1024)(128)(4,1)S(1)}, s32[]{:S(2)}) async-start(s8[8388608]{0:T(1024)(128)(4,1)} %bitcast.175), calls=%async_computation.11 | async-start | bytes 8388608
  165.3 8.0 %slice-start.1 = ((s8[8388608]{0:T(1024)(128)(4,1)}), s8[4194304]{0:T(1024)(128)(4,1)S(1)}, s32[]{:S(2)}) async-start(s8[8388608]{0:T(1024)(128)(4,1)} %bitcast.175), calls=%async_computation.12 | async-start | bytes 8388608
  239.5 111.8 %reduce-scatter.6.cloned.1.call-start = ((), (), s32[]{:S(2)}) async-start(), calls=%async_computation.9 | async-start | bytes 2621440 | tf_op jit(solution)/shard_map/reduce_scatter | solution.py:26
  319.7 51.3 %reduce-scatter.8.cloned.1.call-start = ((), (), s32[]{:S(2)}) async-start(), calls=%async_computation.10 | async-start | bytes 786432 | tf_op jit(solution)/shard_map/reduce_scatter | solution.py:26
  353.2 4.7 %copy-start.1 = (bf16[3,64,32,224]{3,1,2,0:T(8,128)(2,1)S(1)}, bf16[3,64,32,224]{3,1,2,0:T(8,128)(2,1)}, u32[]{:S(2)}) copy-start(bf16[3,64,32,224]{3,1,2,0:T(8,128)(2,1)} %copy.54) | copy-start | bytes 8257540
Sparse Core Ops, SparseCore 0:
  10.5 34.0 all-gather.5
  46.9 29.6 all-gather.3
  78.3 44.9 all-gather.7
  239.6 80.0 reduce-scatter.3
  321.9 29.3 reduce-scatter.5
  354.1 16.8 reduce-scatter.7
